TPU v7x, 32 devices: a whole 2x2x4 slice. The times are simulated.
32 devices in a mesh: ep: 8 (over z, core), tp: 4 (over y, x).
Axes of the slice: x: 2, y: 2, z: 4, core: 2. Of those that a mesh axis runs over, the one named last changes fastest.
Arguments:
- value_in: bfloat16 [8192, 1536], P('ep', 'tp'), may hold values from -6 to 6
- gate_in: bfloat16 [8192, 1536], P('ep', 'tp'), may hold values from -9 to 9
- conv_kernel: float32 [31, 1536], P(None, 'tp'), may hold values from -40 to 40
- norm_gain: float32 [1536], replicated, may hold values from 0.1 to 1.9
- norm_shift: float32 [1536], replicated, may hold values from -3 to 3
- out_weight: bfloat16 [1536, 2048], P(None, 'tp'), may hold values from -0.15625 to 0.15625
- expert_input: bfloat16 [1536, 2048], P('ep'), may hold values from -6 to 6
- expert_gain: float32 [2048], replicated, may hold values from 0.1 to 1.9
- route_ids: int32 [1536, 4], P('ep'), may hold values from 0 to 7, all different within a row; in each aligned block of 192 rows (0 to 191, 192 to 383, ...) at most 120 rows name the same one
- route_weights: float32 [1536, 4], P('ep'), may hold values from 0.2 to 1
- gate_weight: bfloat16 [8, 2048, 2048], P('ep', None, 'tp'), may hold values from -0.375 to 0.375
- up_weight: bfloat16 [8, 2048, 2048], P('ep', None, 'tp'), may hold values from -0.375 to 0.375
- down_weight: bfloat16 [8, 2048, 2048], P('ep', None, 'tp'), may hold values from -0.01953125 to 0.01953125
Outputs:
- mixed_out: bfloat16 [8192, 2048], P('ep', 'tp')
- routed_out: bfloat16 [1536, 2048], P('ep', 'tp')
Inputs may be any that keep to these rules, and one draw needn't show every extreme that they name: `route_ids`: each row names 4 different experts; among the rows of one index of ep (aligned blocks of 192 rows) no expert is named by more than 120 rows, and in some block one expert is named by exactly 120.
All inputs are finite; a program needn't handle non-finite values.
Results may differ from a plain program's by a relative error of at most 0.0071.
Values may be sent and summed in bfloat16 or wider, within the bound.
A program may use at most 64 MiB of HBM per device.

v0:
```python
import jax
import jax.numpy as jnp
from jax import lax
from jax.sharding import PartitionSpec as P


def shifted(block, axis, distance):
    devices = range(lax.axis_size(axis))
    route = [(i - distance, i) for i in devices if i - distance in devices]
    return lax.ppermute(block, axis, route)


def expert_tail(gate_pre, up_pre, down_weight):
    clamped = jnp.minimum(gate_pre, 7.0)
    upward = jnp.clip(up_pre, -7.0, 7.0)
    activation = ((upward + 1.0) * clamped * jax.nn.sigmoid(1.702 * clamped)).astype(jnp.bfloat16)
    weights = down_weight[0]
    summed = jnp.dot(
        lax.all_gather(activation, "tp", axis=1, tiled=True),
        weights,
        preferred_element_type=jnp.float32,
    )
    return summed.astype(jnp.bfloat16)


def finish(gate_pre, up_pre, down_weight, arrived_shape):
    outcome = expert_tail(gate_pre, up_pre, down_weight)
    outcome = outcome.reshape(arrived_shape[0], arrived_shape[1], outcome.shape[1])
    return lax.all_to_all(outcome, "ep", split_axis=0, concat_axis=0, tiled=True)


def body(
    value_in,
    gate_in,
    conv_kernel,
    norm_gain,
    norm_shift,
    out_weight,
    expert_input,
    expert_gain,
    route_ids,
    route_weights,
    gate_weight,
    up_weight,
    down_weight,
):
    gated_values = (
        value_in.astype(jnp.float32) * jax.nn.sigmoid(gate_in.astype(jnp.float32))
    ).astype(jnp.bfloat16)
    kernel_width = conv_kernel.shape[0]
    length_dev = gated_values.shape[0]
    before = shifted(gated_values[length_dev - (kernel_width - 1) :], "ep", 1)
    extended = jnp.concatenate([before, gated_values], 0).astype(jnp.float32)
    running = jnp.zeros(gated_values.shape, jnp.float32)
    for tap_index in range(kernel_width):
        running = (
            running + conv_kernel[tap_index][None, :] * extended[tap_index : tap_index + length_dev]
        )
    convolved = running.astype(jnp.bfloat16)
    gathered = lax.all_gather(convolved, "tp", axis=1, tiled=True).astype(jnp.float32)
    row_mean = jnp.mean(gathered, axis=1, keepdims=True)
    row_var = jnp.mean(jnp.square(gathered - row_mean), axis=1, keepdims=True)
    normed = (gathered - row_mean) * lax.rsqrt(row_var + 1e-05) * norm_gain[None, :] + norm_shift[
        None, :
    ]
    hidden = jax.nn.silu(normed).astype(jnp.bfloat16)
    mixed_out = jnp.dot(hidden, out_weight, preferred_element_type=jnp.float32).astype(jnp.bfloat16)
    experts = lax.axis_size("ep")
    row_count, model_width = expert_input.shape
    top_count = route_ids.shape[1]
    capacity = (5 * row_count * top_count + 4 * experts - 1) // (4 * experts)
    input_float = expert_input.astype(jnp.float32)
    feature_mean = jnp.mean(input_float, axis=1, keepdims=True)
    feature_var = jnp.mean(jnp.square(input_float - feature_mean), axis=1, keepdims=True)
    normed_rows = (
        (input_float - feature_mean) * lax.rsqrt(feature_var + 1e-05) * expert_gain[None, :]
    ).astype(jnp.bfloat16)
    expert_ids = route_ids.reshape(-1)
    onehot = (expert_ids[:, None] == jnp.arange(experts, dtype=jnp.int32)[None, :]).astype(
        jnp.int32
    )
    earlier = jnp.cumsum(onehot, axis=0) - onehot
    position = jnp.sum(earlier * onehot, axis=1)
    destination = expert_ids * capacity + position
    token_index = jnp.arange(expert_ids.shape[0], dtype=jnp.int32) // top_count
    slot_token = (
        jnp.full((experts * capacity,), row_count, jnp.int32).at[destination].set(token_index)
    )
    padded = jnp.concatenate([normed_rows, jnp.zeros((1, model_width), jnp.bfloat16)], 0)
    outgoing = padded[slot_token].reshape(experts, capacity, model_width)
    column_width = model_width // lax.axis_size("tp")
    columns = lax.dynamic_slice_in_dim(
        outgoing, lax.axis_index("tp") * column_width, column_width, 2
    )
    arrived = lax.all_to_all(columns, "ep", split_axis=0, concat_axis=0, tiled=True)
    slot_total = arrived.shape[0] * arrived.shape[1]
    portion = lax.all_gather(arrived, "tp", axis=2, tiled=True)
    flattened = portion.reshape(slot_total, portion.shape[2])
    gate_part = gate_weight[0]
    up_part = up_weight[0]
    gate_pre = jnp.dot(flattened, gate_part, preferred_element_type=jnp.float32)
    up_pre = jnp.dot(flattened, up_part, preferred_element_type=jnp.float32)
    results_home = finish(gate_pre, up_pre, down_weight, arrived.shape)
    picked = results_home.reshape(-1, results_home.shape[2])[destination]
    picked = picked.reshape(row_count, top_count, -1).astype(jnp.float32)
    routed_out = jnp.sum(picked * route_weights[:, :, None], axis=1).astype(jnp.bfloat16)
    return (mixed_out, routed_out)


def solution(mesh):
    return jax.shard_map(
        body,
        mesh=mesh,
        in_specs=(
            P("ep", "tp"),
            P("ep", "tp"),
            P(None, "tp"),
            P(),
            P(),
            P(None, "tp"),
            P("ep", None),
            P(),
            P("ep", None),
            P("ep", None),
            P("ep", None, "tp"),
            P("ep", None, "tp"),
            P("ep", None, "tp"),
        ),
        out_specs=(P("ep", "tp"), P("ep", "tp")),
        check_vma=False,
    )
```

profile of v0, /device:TPU:1, one launch (start us, length us, event | category | flops | bytes accessed | tf_op | source)
XLA Modules:
  0.0 254.0 jit_solution(3363373219548088409)
XLA Ops:
  7.2 0.0 all-gather.6.cloned.1.call-start
  7.2 0.9 copy.19
  8.2 0.1 eq.29
  8.3 0.1 eq.25
  8.4 0.7 broadcast_multiply_fusion
  9.1 1.7 reduce-window.6
  10.8 0.1 slice.296
  10.9 0.1 copy.21
  11.1 0.2 reduce-window.9
  11.2 0.1 copy.22
  11.3 0.1 copy.18
  11.4 0.1 mul.496
  11.5 0.1 fusion.64
  11.7 3.4 %scatter_custom_fusion = s32[960]{0:T(1024)S(1)} fusion(s32[768]{0:T(1024)S(1)} %fusion.69, s32[768]{0:T(1024)S(1)} %add_select_fusion, s32[]{:T(128)} %constant.28.clone.1), kind=kCustom, calls=%fused_computation.118 | custom fusion | bytes 3844 | tf_op jit(solution)/shard_map/scatter | solution.py:87
  15.1 1.3 convert_reduce_fusion.1
  16.4 0.4 fusion.23
  16.8 0.4 fusion.25
  17.2 0.1 concatenate.7
  17.3 5.9 %gather_fusion = bf16[960,2048]{1,0:T(8,128)(2,1)} fusion(bf16[193,2048]{1,0:T(8,128)(2,1)S(1)} %concatenate.7, s32[1024]{0:T(1024)S(1)} %pad_clamp_fusion.1), kind=kCustom, calls=%fused_computation | custom fusion | bytes 7868160 | tf_op jit(solution)/shard_map/gather | solution.py:90
  23.2 1.3 constant_dynamic-slice_fusion
  24.5 30.6 %all_to_all.10 = bf16[8,120,512]{2,1,0:T(8,128)(2,1)} all-to-all(bf16[8,120,512]{2,1,0:T(8,128)(2,1)S(1)} %constant_dynamic-slice_fusion), channel_id=1, replica_groups=mesh['ep'=8,'tp'=4] {'ep'}, dimensions={0} | all-to-all | bytes 1966080 | tf_op jit(solution)/shard_map/all_to_all | solution.py:95
  55.1 0.0 all-gather.6.cloned.1.call-update
  55.1 0.0 all-gather.4.cloned.1.call-start
  55.2 1.6 multiply_convert_fusion.1
  56.8 2.5 collective-permute-start
  59.3 0.1 slice_reduce_fusion.30
  59.4 0.1 slice_reduce_fusion.29
  59.5 0.7 collective-permute-done
  60.2 0.2 maximum_convert_fusion
  60.4 6.8 %fusion.27 = bf16[1024,384]{1,0:T(8,128)(2,1)} fusion(f32[1054,384]{1,0:T(8,128)S(1)} %maximum_convert_fusion, f32[384]{0:T(512)S(1)} %get-tuple-element.31, f32[384]{0:T(512)S(1)} %get-tuple-element.32, f32[384]{0:T(512)S(1)} %get-tuple-element.3, f32[384]{0:T(512)S(1)} %get-tuple-element.4, f32[384]{0:T(512)S(1)} %get-tuple-element.5, ...), kind=kLoop, calls=%fused_computation.33 | loop fusion | flops 24379392 | bytes 49592832 | tf_op jit(solution)/shard_map/convert_element_type | solution.py:59
  67.2 0.0 all-gather.4.cloned.1.call-update
  67.2 0.0 all-gather.8.cloned.1.call-start
  67.3 37.3 %all-gather.6.cloned.1.call-done = bf16[8,120,2048]{2,1,0:T(8,128)(2,1)} async-done(((bf16[8,120,512]{2,1,0:T(8,128)(2,1)}), bf16[8,120,2048]{2,1,0:T(8,128)(2,1)}) %all-gather.6.cloned.1.call-update) | async-done | bytes 3932176 | tf_op jit(solution)/shard_map/all_gather | solution.py:97
  104.6 4.4 %fusion.15 = f32[960,512]{1,0:T(8,128)S(1)} fusion(bf16[960,2048]{1,0:T(8,128)(2,1)} %bitcast.36, bf16[1,2048,512]{2,1,0:T(8,128)(2,1)S(1)} %copy-done), kind=kOutput, calls=%fused_computation.19 | convolution fusion | flops 2013265920 | bytes 7995392 | tf_op jit(solution)/shard_map/dot_general | solution.py:101
  109.1 3.6 %multiply_convert_fusion = bf16[960,512]{1,0:T(8,128)(2,1)} fusion(f32[960,512]{1,0:T(8,128)S(1)} %fusion.15, bf16[960,2048]{1,0:T(8,128)(2,1)S(1)} %bitcast.37, bf16[1,2048,512]{2,1,0:T(8,128)(2,1)S(1)} %copy-done.8), kind=kOutput, calls=%fused_computation.23 | convolution fusion | flops 2018181120 | bytes 8978432 | tf_op jit(solution)/shard_map/dot_general | solution.py:102
  112.7 0.0 all-gather.8.cloned.1.call-update
  112.7 0.1 copy.23
  112.8 37.3 %all-gather.4.cloned.1.call-done = bf16[1024,1536]{1,0:T(8,128)(2,1)} async-done(((bf16[1024,384]{1,0:T(8,128)(2,1)}), bf16[1024,1536]{1,0:T(8,128)(2,1)}) %all-gather.4.cloned.1.call-update) | async-done | bytes 3145744 | tf_op jit(solution)/shard_map/all_gather | solution.py:60
  150.2 2.4 convert_reduce_fusion
  152.5 50.3 %all-gather.8.cloned.1.call-done = bf16[960,2048]{1,0:T(8,128)(2,1)} async-done(((bf16[960,512]{1,0:T(8,128)(2,1)}), bf16[960,2048]{1,0:T(8,128)(2,1)}) %all-gather.8.cloned.1.call-update) | async-done | bytes 3932176 | tf_op jit(solution)/shard_map/all_gather | solution.py:19
  202.9 5.9 %fusion.60 = bf16[960,512]{1,0:T(8,128)(2,1)} fusion(bf16[960,2048]{1,0:T(8,128)(2,1)} %all-gather.8.cloned.1.call-done, bf16[1,2048,512]{2,1,0:T(8,128)(2,1)} %param.25), kind=kOutput, calls=%fused_computation.96 | convolution fusion | flops 2013757440 | bytes 7012352 | tf_op jit(solution)/shard_map/dot_general | solution.py:18
  208.8 5.4 %all-to-all-start.1 = ((bf16[8,120,512]{2,1,0:T(8,128)(2,1)}), bf16[8,120,512]{2,1,0:T(8,128)(2,1)S(1)}, u32[]{:S(2)}, u32[]{:S(2)}) async-start(bf16[8,120,512]{2,1,0:T(8,128)(2,1)} %bitcast.33), calls=%async_computation.1 | async-start | bytes 1966080 | tf_op jit(solution)/shard_map/all_to_all | solution.py:29
  214.2 3.0 %fusion.2 = f32[1024]{0:T(1024)S(1)} fusion(bf16[1024,1536]{1,0:T(8,128)(2,1)} %all-gather.4.cloned.1.call-done, f32[1024]{0:T(1024)S(1)} %broadcast_multiply_fusion.1), kind=kLoop, calls=%fused_computation.7 | loop fusion | flops 6290432 | bytes 3153920 | tf_op jit(solution)/shard_map/reduce_sum | solution.py:62
  217.3 5.2 %fusion.57 = bf16[1024,512]{1,0:T(8,128)(2,1)} fusion(bf16[1536,512]{1,0:T(8,128)(2,1)} %param.18, bf16[1024,1536]{1,0:T(8,128)(2,1)S(1)} %copy-done.1, f32[1536]{0:T(1024)S(1)} %copy-done.9, f32[1536]{0:T(1024)S(1)} %copy-done.10, f32[1024]{0:T(1024)S(1)} %add_rsqrt_fusion, f32[1024]{0:T(1024)S(1)} %broadcast_multiply_fusion.1), kind=kOutput, calls=%fused_computation.95 | convolution fusion | flops 1626865664 | bytes 5787648 | tf_op jit(solution)/shard_map/dot_general | solution.py:67
  222.4 16.0 %all-to-all-done.1 = bf16[8,120,512]{2,1,0:T(8,128)(2,1)S(1)} async-done(((bf16[8,120,512]{2,1,0:T(8,128)(2,1)}), bf16[8,120,512]{2,1,0:T(8,128)(2,1)S(1)}, u32[]{:S(2)}, u32[]{:S(2)}) %all-to-all-start.1) | async-done | bytes 983072 | tf_op jit(solution)/shard_map/all_to_all | solution.py:29
  238.4 3.3 %gather_fusion.1 = bf16[768,512]{1,0:T(8,128)(2,1)} fusion(bf16[960,512]{1,0:T(8,128)(2,1)S(1)} %bitcast.31, s32[1024]{0:T(1024)S(1)} %pad_clamp_fusion), kind=kCustom, calls=%fused_computation.1 | custom fusion | bytes 1575936 | tf_op jit(solution)/shard_map/gather | solution.py:104
  241.8 2.6 %reshape.98 = f32[192,4,512]{2,1,0:T(4,128)} reshape(bf16[768,512]{1,0:T(8,128)(2,1)} %gather_fusion.1) | data formatting | bytes 2359296 | tf_op jit(solution)/shard_map/convert_element_type | solution.py:105
  244.4 3.1 %multiply_reduce_fusion = bf16[192,512]{1,0:T(8,128)(2,1)} fusion(f32[192,4,512]{2,1,0:T(4,128)} %reshape.98, f32[192,4]{1,0:T(8,128)S(1)} %copy.23), kind=kLoop, calls=%fused_computation.93 | loop fusion | flops 688128 | bytes 1772544 | tf_op jit(solution)/shard_map/reduce_sum | solution.py:106
  (33 shorter events, 0.1 us)
Async XLA Ops:
  7.2 97.4 %copy-start = (bf16[1,2048,512]{2,1,0:T(8,128)(2,1)S(1)}, bf16[1,2048,512]{2,1,0:T(8,128)(2,1)}, u32[]{:S(2)}) copy-start(bf16[1,2048,512]{2,1,0:T(8,128)(2,1)} %param.23) | copy-start | bytes 6291460
  7.2 9.2 %copy-start.2 = (bf16[192,2048]{1,0:T(8,128)(2,1)S(1)}, bf16[192,2048]{1,0:T(8,128)(2,1)}, u32[]{:S(2)}) copy-start(bf16[192,2048]{1,0:T(8,128)(2,1)} %param.19) | copy-start | bytes 2359300
  7.2 9.6 %copy-start.5 = (f32[2048]{0:T(1024)S(1)}, f32[2048]{0:T(1024)}, u32[]{:S(2)}) copy-start(f32[2048]{0:T(1024)} %param.20) | copy-start | bytes 24580
  7.2 97.4 %all-gather.6.cloned.1.call-start = ((), (), s32[]{:S(2)}) async-start(), calls=%async_computation.3 | async-start | bytes 4915200 | tf_op jit(solution)/shard_map/all_gather | solution.py:97
  24.5 30.7 %copy-start.3 = (bf16[1024,384]{1,0:T(8,128)(2,1)S(1)}, bf16[1024,384]{1,0:T(8,128)(2,1)}, u32[]{:S(2)}) copy-start(bf16[1024,384]{1,0:T(8,128)(2,1)} %param.14) | copy-start | bytes 2359300
  55.1 4.2 %copy-start.4 = (f32[31,384]{1,0:T(8,128)S(1)}, f32[31,384]{1,0:T(8,128)}, u32[]{:S(2)}) copy-start(f32[31,384]{1,0:T(8,128)} %param.15) | copy-start | bytes 142852
  55.1 95.0 %all-gather.4.cloned.1.call-start = ((), (), s32[]{:S(2)}) async-start(), calls=%async_computation.2 | async-start | bytes 3932160 | tf_op jit(solution)/shard_map/all_gather | solution.py:60
  56.8 3.4 %collective-permute-start = (bf16[30,384]{1,0:T(8,128)(2,1)S(1)}, bf16[30,384]{1,0:T(8,128)(2,1)S(1)}, u32[]{:S(2)}, u32[]{:S(2)}) collective-permute-start(bf16[30,384]{1,0:T(8,128)(2,1)S(1)} %slice.264), channel_id=1, source_target_pairs={{0,4},{4,8},{8,12},{12,16},{16,20},{20,24},{24,28},{1,5},{5,9},{9,... | collective-permute-start | bytes 69128 | tf_op jit(solution)/shard_map/ppermute | solution.py:10
  67.2 135.7 %all-gather.8.cloned.1.call-start = ((), (), s32[]{:S(2)}) async-start(), calls=%async_computation.4 | async-start | bytes 4915200 | tf_op jit(solution)/shard_map/all_gather | solution.py:19
  104.6 4.5 %copy-start.7 = (bf16[8,120,2048]{2,1,0:T(8,128)(2,1)S(1)}, bf16[8,120,2048]{2,1,0:T(8,128)(2,1)}, u32[]{:S(2)}) copy-start(bf16[8,120,2048]{2,1,0:T(8,128)(2,1)} %all-gather.6.cloned.1.call-done) | copy-start | bytes 11796484
  104.6 4.5 %copy-start.8 = (bf16[1,2048,512]{2,1,0:T(8,128)(2,1)S(1)}, bf16[1,2048,512]{2,1,0:T(8,128)(2,1)}, u32[]{:S(2)}) copy-start(bf16[1,2048,512]{2,1,0:T(8,128)(2,1)} %param.24) | copy-start | bytes 6291460
  109.1 3.6 %copy-start.6 = (f32[192,4]{0,1:T(4,128)S(1)}, f32[192,4]{0,1:T(4,128)}, u32[]{:S(2)}) copy-start(f32[192,4]{0,1:T(4,128)} %param.22) | copy-start | bytes 9220
  208.8 29.6 %all-to-all-start.1 = ((bf16[8,120,512]{2,1,0:T(8,128)(2,1)}), bf16[8,120,512]{2,1,0:T(8,128)(2,1)S(1)}, u32[]{:S(2)}, u32[]{:S(2)}) async-start(bf16[8,120,512]{2,1,0:T(8,128)(2,1)} %bitcast.33), calls=%async_computation.1 | async-start | bytes 1966080 | tf_op jit(solution)/shard_map/all_to_all | solution.py:29
  214.2 3.0 %copy-start.1 = (bf16[1024,1536]{1,0:T(8,128)(2,1)S(1)}, bf16[1024,1536]{1,0:T(8,128)(2,1)}, u32[]{:S(2)}) copy-start(bf16[1024,1536]{1,0:T(8,128)(2,1)} %all-gather.4.cloned.1.call-done) | copy-start | bytes 9437188
  214.2 3.0 %copy-start.9 = (f32[1536]{0:T(1024)S(1)}, f32[1536]{0:T(1024)}, u32[]{:S(2)}) copy-start(f32[1536]{0:T(1024)} %param.17) | copy-start | bytes 18436
  214.2 3.0 %copy-start.10 = (f32[1536]{0:T(1024)S(1)}, f32[1536]{0:T(1024)}, u32[]{:S(2)}) copy-start(f32[1536]{0:T(1024)} %param.16) | copy-start | bytes 18436
Sparse Core Ops, SparseCore 0:
  55.3 49.2 all-gather.5
  106.4 43.6 all-gather.3
  152.6 50.2 all-gather.7
where the time goes:
time: 255 us; the launch traced here: 254 us
  waiting for transfers between devices  142 us (56%)
  blocking collectives  30.6 us (12%)
  other arithmetic  21.9 us (9%)
  matrix products  19.1 us (7%)
  local copies, waits for them, and re-layouts  18.6 us (7%)
  between operations  14 us (5%)
  starting transfers between devices  8.07 us (3%)
    all_gather x1, waiting for transfers between devices, expert_tail(): lax.all_gather(activation, 'tp', axis=1, tiled=True)  50.3 us
    all_gather x1, waiting for transfers between devices, body(): portion = lax.all_gather(arrived, 'tp', axis=2, tiled=True)  37.3 us
    all_gather x1, waiting for transfers between devices, body(): lax.all_gather(convolved, 'tp', axis=1, tiled=True).astype(jnp.float32)  37.3 us
    all_to_all x1, blocking collectives, body(): lax.all_to_all(columns, 'ep', split_axis=0, concat_axis=0, tiled=True)  30.6 us
    all_to_all x1, waiting for transfers between devices, finish(): lax.all_to_all(outcome, 'ep', split_axis=0, concat_axis=0, tiled=True)  16 us
    convert_element_type x1, other arithmetic, body(): convolved = running.astype(jnp.bfloat16)  6.79 us
    dot_general x1, matrix products, expert_tail(): jnp.dot(lax.all_gather(activation, 'tp', axis=1, tiled=True), weights, pr...  5.93 us
    gather x1, local copies, waits for them, and re-layouts, body(): outgoing = padded[slot_token].reshape(experts, capacity, model_width)  5.91 us
  transfers between devices with their start and end apart: 5, of which 5 were waited for; matrix products, arithmetic and copies ran while one was open for 11% of the time, Pallas kernels for 0%

commit v1 on v0

--- a/solution.py
+++ b/solution.py
@@ -1,7 +1,421 @@
+import functools
+
 import jax
 import jax.numpy as jnp
 from jax import lax
+from jax.experimental import pallas as pl
+from jax.experimental.pallas import tpu as pltpu
 from jax.sharding import PartitionSpec as P
+
+MESH = pl.DeviceIdType.MESH
+F32 = jnp.float32
+BF16 = jnp.bfloat16
+HALO = 32
+
+
+def up_to(value, step):
+    return (value + step - 1) // step * step
+
+
+def half_sigmoid(v):
+    return 0.5 + 0.5 * jnp.tanh(0.5 * v)
+
+
+def kernel(
+    cfg,
+    value_ref,
+    gate_ref,
+    taps_ref,
+    gain_ref,
+    shift_ref,
+    rows_ref,
+    row_gain_ref,
+    ids_ref,
+    ids_t_ref,
+    route_w_ref,
+    out_w_hbm,
+    gate_w_hbm,
+    up_w_hbm,
+    down_w_hbm,
+    mixed_ref,
+    routed_ref,
+    ext,
+    conv,
+    hidden,
+    rows_all,
+    slots,
+    acts,
+    res,
+    ret,
+    out_w,
+    gate_w,
+    up_w,
+    down_w,
+    w_sem,
+    halo_sem,
+    conv_s,
+    conv_r,
+    rows_s,
+    rows_r,
+    act_s,
+    act_r,
+    ret_s,
+    ret_r,
+):
+    n_ep, n_tp, taps, nk, slot, experts = cfg
+    n_z = n_ep // 2
+    me = lax.axis_index("ep")
+    t = lax.axis_index("tp")
+    p = me // 2
+    c = me % 2
+    tx = t + 1 - 2 * (t % 2)
+    ty = t + 2 - 4 * (t // 2)
+    td = 3 - t
+    length, ch = value_ref.shape
+    groups = ch // 128
+    n_rows, width = rows_ref.shape
+    half_ff = gate_w.shape[1]
+    cols_out = out_w.shape[1]
+    chunk = length // nk
+    tile = 256
+    pending = []
+
+    loads = []
+    for i, (src, dst) in enumerate(
+        ((gate_w_hbm.at[0], gate_w), (up_w_hbm.at[0], up_w), (out_w_hbm, out_w), (down_w_hbm.at[0], down_w))
+    ):
+        copy = pltpu.make_async_copy(src, dst, w_sem.at[i])
+        copy.start()
+        loads.append(copy)
+
+    barrier = pltpu.get_barrier_semaphore()
+    for i in range(1, n_ep):
+        pl.semaphore_signal(
+            barrier, inc=1, device_id={"ep": (me + i) % n_ep}, device_id_type=MESH
+        )
+    for other in (tx, ty):
+        pl.semaphore_signal(barrier, inc=1, device_id={"tp": other}, device_id_type=MESH)
+
+    def send(src, dst, ss, rs, dev, cond=None):
+        def make():
+            return pltpu.make_async_remote_copy(
+                src_ref=src,
+                dst_ref=dst,
+                send_sem=ss,
+                recv_sem=rs,
+                device_id=dev,
+                device_id_type=MESH,
+            )
+
+        if cond is None:
+            make().start()
+        else:
+
+            @pl.when(cond)
+            def _():
+                make().start()
+
+        pending.append((make, cond))
+
+    def arrived(ref, ss, rs, cond=None):
+        def wait():
+            pltpu.make_async_remote_copy(
+                src_ref=ref,
+                dst_ref=ref,
+                send_sem=ss,
+                recv_sem=rs,
+                device_id={"tp": tx},
+                device_id_type=MESH,
+            ).wait_recv()
+
+        if cond is None:
+            wait()
+        else:
+            pl.when(cond)(wait)
+
+    def gated_step(i, _):
+        r = pl.multiple_of(i * 32, 32)
+        for g in range(groups):
+            lanes = slice(g * 128, (g + 1) * 128)
+            v = value_ref[pl.ds(r, 32), lanes].astype(F32)
+            s = half_sigmoid(gate_ref[pl.ds(r, 32), lanes].astype(F32))
+            ext[g, pl.ds(HALO + r, 32), :] = (v * s).astype(BF16).astype(F32)
+        return 0
+
+    lax.fori_loop(0, length // 32, gated_step, 0)
+
+    def norm_step(i, _):
+        r = pl.multiple_of(i * 16, 16)
+        x = rows_ref[pl.ds(r, 16), :].astype(F32)
+        mean = jnp.mean(x, axis=1, keepdims=True)
+        d = x - mean
+        var = jnp.mean(d * d, axis=1, keepdims=True)
+        rows_all[p, c, pl.ds(r, 16), :] = (d * lax.rsqrt(var + 1e-05) * row_gain_ref[...]).astype(BF16)
+        return 0
+
+    lax.fori_loop(0, n_rows // 16, norm_step, 0)
+    extra = rows_all.shape[2] - n_rows
+    lanes_t = ids_t_ref.shape[1]
+    e_iota = lax.broadcasted_iota(jnp.int32, (extra, lanes_t), 0)
+    named_t = jnp.zeros((extra, lanes_t), F32)
+    for k in range(ids_t_ref.shape[0]):
+        named_t += jnp.where(ids_t_ref[k : k + 1, :] == e_iota, 1.0, 0.0)
+    before_t = jnp.where(
+        lax.broadcasted_iota(jnp.int32, (lanes_t, lanes_t), 0)
+        < lax.broadcasted_iota(jnp.int32, (lanes_t, lanes_t), 1),
+        1.0,
+        0.0,
+    ).astype(BF16)
+    pos_t = jnp.dot(named_t.astype(BF16), before_t, preferred_element_type=F32)
+    rows_all[p, c, n_rows : n_rows + extra, :] = jnp.zeros((extra, width), BF16)
+    rows_all[p, c, n_rows : n_rows + extra, 0:lanes_t] = jnp.where(named_t > 0.5, pos_t, -1.0).astype(BF16)
+
+    pl.semaphore_wait(barrier, n_ep - 1 + 2)
+
+    tail = ext.at[:, pl.ds(length, HALO), :]
+    head = ext.at[:, pl.ds(0, HALO), :]
+    send(tail, head, halo_sem.at[0], halo_sem.at[1], {"ep": (me + 1) % n_ep}, me < n_ep - 1)
+
+    def send_rows(q, up, down):
+        block = rows_all.at[q, c]
+        send(block, block, rows_s.at[q, 0], rows_r.at[q, c], {"ep": (me + 2) % n_ep}, up)
+        send(block, block, rows_s.at[q, 1], rows_r.at[q, c], {"ep": (me + n_ep - 2) % n_ep}, down)
+        exists = jnp.logical_or(up, down)
+        return block, exists
+
+    def to_partner(q, cond):
+        block = rows_all.at[q, c]
+        send(block, block, rows_s.at[q, 2], rows_r.at[q, c], {"ep": me + 1 - 2 * c}, cond)
+
+    send_rows(p, p < n_z - 1, p > 0)
+    to_partner(p, None)
+
+    @pl.when(me == 0)
+    def _():
+        ext[:, 0:HALO, :] = jnp.zeros((groups, HALO, 128), F32)
+
+    def conv_chunk(k):
+        for g in range(groups):
+            lanes = slice(g * 128, (g + 1) * 128)
+            weights = [taps_ref[j : j + 1, lanes] for j in range(taps)]
+
+            def step(i, _):
+                r = pl.multiple_of(k * chunk + i * 64, 64)
+                total = weights[0] * ext[g, pl.ds(r + HALO - taps + 1, 64), :]
+                for j in range(1, taps):
+                    total += weights[j] * ext[g, pl.ds(r + HALO - taps + 1 + j, 64), :]
+                conv[t, pl.ds(r, 64), lanes] = total.astype(BF16)
+                return 0
+
+            lax.fori_loop(0, chunk // 64, step, 0)
+        part = conv.at[t, pl.ds(k * chunk, chunk), :]
+        send(part, part, conv_s.at[0, k], conv_r.at[t, k], {"tp": tx})
+        send(part, part, conv_s.at[1, k], conv_r.at[t, k], {"tp": ty})
+
+    order = list(range(1, nk)) + [0]
+    for k in order:
+        if k == 0:
+            arrived(head, halo_sem.at[0], halo_sem.at[1], me > 0)
+        conv_chunk(k)
+
+    def conv_relay(k):
+        rows = pl.ds(k * chunk, chunk)
+        for source in (tx, ty):
+            arrived(conv.at[source, rows, :], conv_s.at[0, k], conv_r.at[source, k])
+        source, target = (tx, ty) if k % 2 == 0 else (ty, tx)
+        part = conv.at[source, rows, :]
+        send(part, part, conv_s.at[2, k], conv_r.at[source, k], {"tp": target})
+
+    def project(k):
+        arrived(conv.at[td, pl.ds(k * chunk, chunk), :], conv_s.at[0, k], conv_r.at[td, k])
+
+        def step(i, _):
+            r = pl.multiple_of(k * chunk + i * 16, 16)
+            h = pl.multiple_of(i * 16, 16)
+            parts = [conv[u, pl.ds(r, 16), :].astype(F32) for u in range(n_tp)]
+            mean = sum(jnp.sum(x, axis=1, keepdims=True) for x in parts) / (n_tp * ch)
+            parts = [x - mean for x in parts]
+            var = sum(jnp.sum(x * x, axis=1, keepdims=True) for x in parts) / (n_tp * ch)
+            scale = lax.rsqrt(var + 1e-05)
+            for u in range(n_tp):
+                v = parts[u] * scale * gain_ref[u : u + 1, :] + shift_ref[u : u + 1, :]
+                hidden[pl.ds(h, 16), u * ch : (u + 1) * ch] = (v * half_sigmoid(v)).astype(BF16)
+            return 0
+
+        lax.fori_loop(0, chunk // 16, step, 0, unroll=2)
+
+        def cols(i, _):
+            o = pl.multiple_of(i * tile, tile)
+            mixed_ref[k * chunk : (k + 1) * chunk, pl.ds(o, tile)] = jnp.dot(
+                hidden[...], out_w[:, pl.ds(o, tile)], preferred_element_type=F32
+            ).astype(BF16)
+            return 0
+
+        lax.fori_loop(0, cols_out // tile, cols, 0)
+
+    less = jnp.minimum(p, n_z - 1 - p)
+    longer_up = jnp.where(p <= n_z - 1 - p, 1, -1)
+
+    def chip_of(j):
+        near = p + (j + 1) // 2 * (-1 if j % 2 else 1)
+        return jnp.where(j <= 2 * less, near, p + longer_up * (j - less))
+
+    def rows_relay(d):
+        below, above = p - d, p + d
+        low = jnp.maximum(below, 0)
+        high = jnp.minimum(above, n_z - 1)
+        has_low, has_high = below >= 0, above <= n_z - 1
+        for q, has, step, onward in (
+            (low, has_low, 2, jnp.logical_and(has_low, p < n_z - 1)),
+            (high, has_high, n_ep - 2, jnp.logical_and(has_high, p > 0)),
+        ):
+            block = rows_all.at[q, c]
+            arrived(block, rows_s.at[q, 0], rows_r.at[q, c], has)
+            send(block, block, rows_s.at[q, 0], rows_r.at[q, c], {"ep": (me + step) % n_ep}, onward)
+            to_partner(q, has)
+
+    def act_part(source, q, h):
+        return acts.at[source, q, pl.ds(h * slot, slot), :]
+
+    def expert_up(j):
+        q = chip_of(j)
+        arrived(rows_all.at[q, 1 - c], rows_s.at[q, 0], rows_r.at[q, 1 - c])
+        for h in range(2):
+            marks = rows_all[q, h, n_rows : n_rows + extra, 0:lanes_t].astype(F32)
+            mine = jnp.sum(jnp.where(e_iota == me, marks, 0.0), axis=0, keepdims=True)[:, :n_rows]
+            pick = jnp.where(
+                lax.broadcasted_iota(jnp.int32, (slot, n_rows), 0).astype(F32) == mine, 1.0, 0.0
+            ).astype(BF16)
+
+            def gather(i, _):
+                o = pl.multiple_of(i * tile, tile)
+                slots[h * slot : (h + 1) * slot, pl.ds(o, tile)] = jnp.dot(
+                    pick, rows_all[q, h, 0:n_rows, pl.ds(o, tile)], preferred_element_type=F32
+                ).astype(BF16)
+                return 0
+
+            lax.fori_loop(0, width // tile, gather, 0)
+        if j == 0:
+            loads[0].wait()
+            loads[1].wait()
+
+        def cols(i, _):
+            o = pl.multiple_of(i * tile, tile)
+            x = slots[...]
+            gate = jnp.dot(x, gate_w[:, pl.ds(o, tile)], preferred_element_type=F32)
+            up = jnp.dot(x, up_w[:, pl.ds(o, tile)], preferred_element_type=F32)
+            gate = jnp.minimum(gate, 7.0)
+            up = jnp.clip(up, -7.0, 7.0)
+            acts[t, q, :, pl.ds(o, tile)] = ((up + 1.0) * gate * half_sigmoid(1.702 * gate)).astype(BF16)
+            return 0
+
+        lax.fori_loop(0, half_ff // tile, cols, 0)
+        for h in range(2):
+            part = act_part(t, q, h)
+            send(part, part, act_s.at[0, q, h], act_r.at[t, q, h], {"tp": tx})
+            send(part, part, act_s.at[1, q, h], act_r.at[t, q, h], {"tp": ty})
+
+    def act_relay(j):
+        q = chip_of(j)
+        for h, source, target in ((0, tx, ty), (1, ty, tx)):
+            part = act_part(source, q, h)
+            arrived(part, act_s.at[0, q, h], act_r.at[source, q, h])
+            send(part, part, act_s.at[2, q, h], act_r.at[source, q, h], {"tp": target})
+
+    def expert_down(j):
+        q = chip_of(j)
+        for source, h in ((tx, 1), (ty, 0), (td, 0), (td, 1)):
+            arrived(act_part(source, q, h), act_s.at[0, q, h], act_r.at[source, q, h])
+        if j == 0:
+            loads[3].wait()
+
+        def cols(i, _):
+            o = pl.multiple_of(i * tile, tile)
+            total = jnp.zeros((2 * slot, tile), F32)
+            for u in range(n_tp):
+                total += jnp.dot(
+                    acts[u, q],
+                    down_w[u * half_ff : (u + 1) * half_ff, pl.ds(o, tile)],
+                    preferred_element_type=F32,
+                )
+            res[q, :, pl.ds(o, tile)] = total.astype(BF16)
+            return 0
+
+        lax.fori_loop(0, cols_out // tile, cols, 0)
+        for h in range(2):
+            target = 2 * q + h
+            part = res.at[q, pl.ds(h * slot, slot), :]
+            send(part, ret.at[me], ret_s.at[target], ret_r.at[me], {"ep": target}, target != me)
+        if j == 0:
+            for h in range(2):
+
+                @pl.when(c == h)
+                def _():
+                    ret[me] = res[p, h * slot : (h + 1) * slot, :]
+
+    expert_up(0)
+    half = nk // 2
+    for k in order[:half]:
+        conv_relay(k)
+    if n_z > 1:
+        rows_relay(1)
+        expert_up(1)
+    for k in order[half:]:
+        conv_relay(k)
+    act_relay(0)
+    loads[2].wait()
+    waiting = list(order)
+    for _ in range(half):
+        project(waiting.pop(0))
+    if n_z > 1:
+        act_relay(1)
+    for j in range(2, n_z):
+        rows_relay(j)
+        expert_up(j)
+        if waiting:
+            project(waiting.pop(0))
+        expert_down(j - 2)
+        act_relay(j)
+    for k in waiting:
+        project(k)
+    for j in range(max(0, n_z - 2), n_z):
+        expert_down(j)
+
+    lane_e = lax.broadcasted_iota(jnp.int32, (n_rows, 128), 1)
+    named = jnp.zeros((n_rows, 128), F32)
+    share = jnp.zeros((n_rows, 128), F32)
+    for k in range(ids_ref.shape[1]):
+        hit = ids_ref[:, k : k + 1] == lane_e
+        named += jnp.where(hit, 1.0, 0.0)
+        share += jnp.where(hit, route_w_ref[:, k : k + 1], 0.0)
+    before = jnp.where(
+        lax.broadcasted_iota(jnp.int32, (n_rows, n_rows), 1)
+        < lax.broadcasted_iota(jnp.int32, (n_rows, n_rows), 0),
+        1.0,
+        0.0,
+    ).astype(BF16)
+    pos = jnp.dot(before, named.astype(BF16), preferred_element_type=F32)
+    pos = jnp.where(named > 0.5, pos, -1.0)
+    slot_iota = lax.broadcasted_iota(jnp.int32, (n_rows, slot), 1).astype(F32)
+    total = jnp.zeros((n_rows, cols_out), F32)
+    for e in range(experts):
+        arrived(ret.at[e], ret_s.at[e], ret_r.at[e], me != e)
+        combine = jnp.where(pos[:, e : e + 1] == slot_iota, share[:, e : e + 1], 0.0)
+        high = combine.astype(BF16)
+        low = (combine - high.astype(F32)).astype(BF16)
+        back = ret[e]
+        total += jnp.dot(high, back, preferred_element_type=F32)
+        total += jnp.dot(low, back, preferred_element_type=F32)
+    routed_ref[...] = total.astype(BF16)
+
+    for make, cond in pending:
+        if cond is None:
+            make().wait_send()
+        else:
+
+            @pl.when(cond)
+            def _(make=make):
+                make().wait_send()
 
 
 def shifted(block, axis, distance):
@@ -29,7 +443,7 @@
     return lax.all_to_all(outcome, "ep", split_axis=0, concat_axis=0, tiled=True)
 
 
-def body(
+def plain_body(
     value_in,
     gate_in,
     conv_kernel,
@@ -107,6 +521,108 @@
     return (mixed_out, routed_out)
 
 
+def body(
+    value_in,
+    gate_in,
+    conv_kernel,
+    norm_gain,
+    norm_shift,
+    out_weight,
+    expert_input,
+    expert_gain,
+    route_ids,
+    route_weights,
+    gate_weight,
+    up_weight,
+    down_weight,
+):
+    n_ep, n_tp = lax.axis_size("ep"), lax.axis_size("tp")
+    length, ch = value_in.shape
+    n_rows, width = expert_input.shape
+    top = route_ids.shape[1]
+    if n_tp != 4 or ch % 128 or n_ep % 2:
+        return plain_body(
+            value_in,
+            gate_in,
+            conv_kernel,
+            norm_gain,
+            norm_shift,
+            out_weight,
+            expert_input,
+            expert_gain,
+            route_ids,
+            route_weights,
+            gate_weight,
+            up_weight,
+            down_weight,
+        )
+    experts = n_ep
+    capacity = (5 * n_rows * top + 4 * experts - 1) // (4 * experts)
+    slot = up_to(capacity, 16)
+    extra = up_to(experts, 16)
+    half_ff = gate_weight.shape[2]
+    cols_out = out_weight.shape[1]
+    down_cols = down_weight.shape[2]
+    nk = 4
+    n_z = n_ep // 2
+    ids_t = jnp.pad(route_ids.T, ((0, 0), (0, up_to(n_rows, 128) - n_rows)), constant_values=-1)
+    cfg = (n_ep, n_tp, conv_kernel.shape[0], nk, slot, experts)
+    vmem = pl.BlockSpec(memory_space=pltpu.VMEM)
+    hbm = pl.BlockSpec(memory_space=pl.ANY)
+    dma = pltpu.SemaphoreType.DMA
+    return pl.pallas_call(
+        functools.partial(kernel, cfg),
+        out_shape=(
+            jax.ShapeDtypeStruct((length, cols_out), BF16),
+            jax.ShapeDtypeStruct((n_rows, down_cols), BF16),
+        ),
+        in_specs=[vmem] * 10 + [hbm] * 4,
+        out_specs=(vmem, vmem),
+        scratch_shapes=[
+            pltpu.VMEM((ch // 128, HALO + length, 128), F32),
+            pltpu.VMEM((n_tp, length, ch), BF16),
+            pltpu.VMEM((length // nk, n_tp * ch), BF16),
+            pltpu.VMEM((n_z, 2, n_rows + extra, width), BF16),
+            pltpu.VMEM((2 * slot, width), BF16),
+            pltpu.VMEM((n_tp, n_z, 2 * slot, half_ff), BF16),
+            pltpu.VMEM((n_z, 2 * slot, down_cols), BF16),
+            pltpu.VMEM((n_ep, slot, down_cols), BF16),
+            pltpu.VMEM(out_weight.shape, BF16),
+            pltpu.VMEM(gate_weight.shape[1:], BF16),
+            pltpu.VMEM(up_weight.shape[1:], BF16),
+            pltpu.VMEM(down_weight.shape[1:], BF16),
+            dma((4,)),
+            dma((2,)),
+            dma((3, nk)),
+            dma((n_tp, nk)),
+            dma((n_z, 3)),
+            dma((n_z, 2)),
+            dma((3, n_z, 2)),
+            dma((n_tp, n_z, 2)),
+            dma((n_ep,)),
+            dma((n_ep,)),
+        ],
+        compiler_params=pltpu.CompilerParams(
+            collective_id=0, has_side_effects=True, vmem_limit_bytes=62 * 1024 * 1024
+        ),
+    )(
+        value_in,
+        gate_in,
+        conv_kernel,
+        norm_gain.reshape(n_tp, ch),
+        norm_shift.reshape(n_tp, ch),
+        expert_input,
+        expert_gain.reshape(1, width),
+        route_ids,
+        ids_t,
+        route_weights,
+        out_weight,
+        gate_weight,
+        up_weight,
+        down_weight,
+    )
+
+
 def solution(mesh):
     return jax.shard_map(
         body,

time: 255 us -> 109 us (0.43)
  waiting for transfers between devices: 142 us -> 0 us
  Pallas kernels: 0 us -> 98.2 us
  blocking collectives: 30.6 us -> 0 us
  other arithmetic: 21.9 us -> 0 us
  matrix products: 19.1 us -> 0 us
  between operations: 14 us -> 0.65 us
  local copies, waits for them, and re-layouts: 18.6 us -> 9.76 us
  starting transfers between devices: 8.07 us -> 0 us
    all_gather x3 -> x0, waiting for transfers between devices: 125 us -> none  [the longest x1 50.3 us: expert_tail(): lax.all_gather(activation, 'tp', axis=1, tiled=True)]
    pallas_call x0 -> x1, Pallas kernels: none -> 98.2 us  [body(): pl.pallas_call(functools.partial(kernel, cfg), out_shape=(jax.ShapeDtypeS...]
    all_to_all x1 -> x0, blocking collectives: 30.6 us -> none  [body(): lax.all_to_all(columns, 'ep', split_axis=0, concat_axis=0, tiled=True)]
    dot_general x4 -> x0, matrix products: 19.1 us -> none  [the longest x1 5.93 us: expert_tail(): jnp.dot(lax.all_gather(activation, 'tp', axis=1, tiled=True), weights, pr...]
    all_to_all x1 -> x0, waiting for transfers between devices: 16 us -> none  [finish(): lax.all_to_all(outcome, 'ep', split_axis=0, concat_axis=0, tiled=True)]
    reduce_sum x6 -> x0, other arithmetic: 10.3 us -> none  [the longest x1 3.14 us: body(): jnp.sum(picked * route_weights[:, :, None], axis=1).astype(jnp.bfloat16)]
    gather x2 -> x0, local copies, waits for them, and re-layouts: 9.24 us -> none  [the longest x1 5.91 us: body(): outgoing = padded[slot_token].reshape(experts, capacity, model_width)]
    convert_element_type x5 -> x0, other arithmetic: 8.96 us -> none  [the longest x1 6.79 us: body(): convolved = running.astype(jnp.bfloat16)]
  transfers between devices with their start and end apart: 5 -> 0, of which waited for: 5 -> 0; matrix products, arithmetic and copies ran while one was open for 11% -> 0% of each run, Pallas kernels for 0% -> 0%
where the time goes in v1:
time: 109 us
  Pallas kernels  98.2 us (90%)
  local copies, waits for them, and re-layouts  9.76 us (9%)
    pallas_call x1, Pallas kernels, body(): pl.pallas_call(functools.partial(kernel, cfg), out_shape=(jax.ShapeDtypeS...  98.2 us
    unnamed x6, local copies, waits for them, and re-layouts  5.88 us

profile of v1, /device:TPU:1, one launch (start us, length us, event | category | flops | bytes accessed | tf_op | source)
XLA Modules:
  0.0 108.6 jit_solution(10683382654335115003)
XLA Ops:
  0.6 1.3 %pad.4.ids_t_ref = s32[4,256]{1,0:T(4,128)} pad(s32[4,192]{1,0:T(4,128)} %bitcast.2, s32[]{:T(128)} %constant.0.clone.1), padding=0_0x0_64 | pad | bytes 7172 | tf_op jit(solution)/shard_map/jit(_pad)/pad | solution.py:568
  1.9 1.3 %reshape.13.gain_ref = f32[4,384]{1,0:T(4,128)} reshape(f32[1536]{0:T(1024)} %param.16) | data formatting | bytes 12288 | tf_op jit(solution)/shard_map/reshape | solution.py:612
  3.2 1.3 %reshape.14.shift_ref = f32[4,384]{1,0:T(4,128)} reshape(f32[1536]{0:T(1024)} %param.17) | data formatting | bytes 12288 | tf_op jit(solution)/shard_map/reshape | solution.py:613
  4.5 1.4 %copy.16.route_w_ref = f32[192,4]{1,0:T(8,128)} copy(f32[192,4]{0,1:T(4,128)} %param.22) | data formatting | bytes 6144 | tf_op args[9]
  6.0 1.4 %copy.15.ids_ref = s32[192,4]{1,0:T(8,128)} copy(s32[192,4]{0,1:T(4,128)} %param.21) | data formatting | bytes 6144 | tf_op args[8]
  7.4 98.2 %shard_map.140 = (bf16[1024,512]{1,0:T(8,128)(2,1)}, bf16[192,512]{1,0:T(8,128)(2,1)}) custom-call(bf16[1024,384]{1,0:T(8,128)(2,1)} %value_ref.1, bf16[1024,384]{1,0:T(8,128)(2,1)} %gate_ref.1, f32[31,384]{1,0:T(8,128)} %taps_ref.1, f32[4,384]{1,0:T(4,128)} %reshape.13.gain_ref, f32[4,384]{1,0:T(4,128)} %reshape.14.shift_ref, bf16[192,2048]{1,0:T(8,128)(2,1)} %rows_ref.1, ...), custom_call_target="tpu_custom_call" | custom-call | tf_op jit(solution)/shard_map/pallas_call | solution.py:573
  105.6 0.0 copy-start
  105.6 2.3 %copy.19 = bf16[1024,512]{1,0:T(8,128)(2,1)} copy(bf16[1024,512]{1,0:T(8,128)(2,1)} %get-tuple-element.4) | data formatting | bytes 2097152
  107.9 0.0 copy-done
  107.9 0.7 copy.20
Async XLA Ops:
  105.6 2.3 %copy-start = (bf16[192,512]{1,0:T(8,128)(2,1)S(1)}, bf16[192,512]{1,0:T(8,128)(2,1)}, u32[]{:S(2)}) copy-start(bf16[192,512]{1,0:T(8,128)(2,1)} %get-tuple-element.5) | copy-start | bytes 589828

commit v2 on v1

--- a/solution.py
+++ b/solution.py
@@ -30,7 +30,6 @@
     shift_ref,
     rows_ref,
     row_gain_ref,
-    ids_ref,
     ids_t_ref,
     route_w_ref,
     out_w_hbm,
@@ -43,6 +42,8 @@
     conv,
     hidden,
     rows_all,
+    marks_all,
+    route_t,
     slots,
     acts,
     res,
@@ -57,6 +58,8 @@
     conv_r,
     rows_s,
     rows_r,
+    mark_s,
+    mark_r,
     act_s,
     act_r,
     ret_s,
@@ -154,27 +157,36 @@
         return 0
 
     lax.fori_loop(0, n_rows // 16, norm_step, 0)
-    extra = rows_all.shape[2] - n_rows
-    lanes_t = ids_t_ref.shape[1]
-    e_iota = lax.broadcasted_iota(jnp.int32, (extra, lanes_t), 0)
-    named_t = jnp.zeros((extra, lanes_t), F32)
+    extra = marks_all.shape[1]
+    e_iota = lax.broadcasted_iota(jnp.int32, (extra, n_rows), 0)
+    named_t = jnp.zeros((extra, n_rows), F32)
+    share_t = jnp.zeros((extra, n_rows), F32)
     for k in range(ids_t_ref.shape[0]):
-        named_t += jnp.where(ids_t_ref[k : k + 1, :] == e_iota, 1.0, 0.0)
+        hit = ids_t_ref[k : k + 1, :] == e_iota
+        named_t += jnp.where(hit, 1.0, 0.0)
+        share_t += jnp.where(hit, route_w_ref[k : k + 1, :], 0.0)
     before_t = jnp.where(
-        lax.broadcasted_iota(jnp.int32, (lanes_t, lanes_t), 0)
-        < lax.broadcasted_iota(jnp.int32, (lanes_t, lanes_t), 1),
+        lax.broadcasted_iota(jnp.int32, (n_rows, n_rows), 0)
+        < lax.broadcasted_iota(jnp.int32, (n_rows, n_rows), 1),
         1.0,
         0.0,
     ).astype(BF16)
     pos_t = jnp.dot(named_t.astype(BF16), before_t, preferred_element_type=F32)
-    rows_all[p, c, n_rows : n_rows + extra, :] = jnp.zeros((extra, width), BF16)
-    rows_all[p, c, n_rows : n_rows + extra, 0:lanes_t] = jnp.where(named_t > 0.5, pos_t, -1.0).astype(BF16)
+    pos_t = jnp.where(named_t > 0.5, pos_t, -1.0)
+    marks_all[me] = pos_t.astype(BF16)
+    route_t[0] = pos_t
+    route_t[1] = share_t
 
     pl.semaphore_wait(barrier, n_ep - 1 + 2)
 
     tail = ext.at[:, pl.ds(length, HALO), :]
     head = ext.at[:, pl.ds(0, HALO), :]
     send(tail, head, halo_sem.at[0], halo_sem.at[1], {"ep": (me + 1) % n_ep}, me < n_ep - 1)
+
+    for i in range(1, n_ep):
+        other = (me + i) % n_ep
+        mark = marks_all.at[me]
+        send(mark, mark, mark_s.at[other], mark_r.at[me], {"ep": other})
 
     def send_rows(q, up, down):
         block = rows_all.at[q, c]
@@ -238,7 +250,7 @@
             var = sum(jnp.sum(x * x, axis=1, keepdims=True) for x in parts) / (n_tp * ch)
             scale = lax.rsqrt(var + 1e-05)
             for u in range(n_tp):
-                v = parts[u] * scale * gain_ref[u : u + 1, :] + shift_ref[u : u + 1, :]
+                v = parts[u] * scale * gain_ref[:, u * ch : (u + 1) * ch] + shift_ref[:, u * ch : (u + 1) * ch]
                 hidden[pl.ds(h, 16), u * ch : (u + 1) * ch] = (v * half_sigmoid(v)).astype(BF16)
             return 0
 
@@ -281,8 +293,10 @@
         q = chip_of(j)
         arrived(rows_all.at[q, 1 - c], rows_s.at[q, 0], rows_r.at[q, 1 - c])
         for h in range(2):
-            marks = rows_all[q, h, n_rows : n_rows + extra, 0:lanes_t].astype(F32)
-            mine = jnp.sum(jnp.where(e_iota == me, marks, 0.0), axis=0, keepdims=True)[:, :n_rows]
+            owner = 2 * q + h
+            arrived(marks_all.at[owner], mark_s.at[owner], mark_r.at[owner], owner != me)
+            marks = marks_all[owner].astype(F32)
+            mine = jnp.sum(jnp.where(e_iota == me, marks, 0.0), axis=0, keepdims=True)
             pick = jnp.where(
                 lax.broadcasted_iota(jnp.int32, (slot, n_rows), 0).astype(F32) == mine, 1.0, 0.0
             ).astype(BF16)
@@ -365,47 +379,39 @@
     act_relay(0)
     loads[2].wait()
     waiting = list(order)
-    for _ in range(half):
-        project(waiting.pop(0))
+    project(waiting.pop(0))
     if n_z > 1:
         act_relay(1)
+    done = 0
     for j in range(2, n_z):
         rows_relay(j)
         expert_up(j)
-        if waiting:
-            project(waiting.pop(0))
-        expert_down(j - 2)
+        if j + 1 < n_z:
+            while waiting:
+                project(waiting.pop(0))
+                if done < j:
+                    expert_down(done)
+                    done += 1
         act_relay(j)
-    for k in waiting:
-        project(k)
-    for j in range(max(0, n_z - 2), n_z):
+        while done < j + 1:
+            expert_down(done)
+            done += 1
+    while waiting:
+        project(waiting.pop(0))
+    for j in range(done, n_z):
         expert_down(j)
 
-    lane_e = lax.broadcasted_iota(jnp.int32, (n_rows, 128), 1)
-    named = jnp.zeros((n_rows, 128), F32)
-    share = jnp.zeros((n_rows, 128), F32)
-    for k in range(ids_ref.shape[1]):
-        hit = ids_ref[:, k : k + 1] == lane_e
-        named += jnp.where(hit, 1.0, 0.0)
-        share += jnp.where(hit, route_w_ref[:, k : k + 1], 0.0)
-    before = jnp.where(
-        lax.broadcasted_iota(jnp.int32, (n_rows, n_rows), 1)
-        < lax.broadcasted_iota(jnp.int32, (n_rows, n_rows), 0),
-        1.0,
-        0.0,
-    ).astype(BF16)
-    pos = jnp.dot(before, named.astype(BF16), preferred_element_type=F32)
-    pos = jnp.where(named > 0.5, pos, -1.0)
-    slot_iota = lax.broadcasted_iota(jnp.int32, (n_rows, slot), 1).astype(F32)
+    slot_iota = lax.broadcasted_iota(jnp.int32, (slot, n_rows), 0).astype(F32)
+    over_slots = (((0,), (0,)), ((), ()))
     total = jnp.zeros((n_rows, cols_out), F32)
     for e in range(experts):
         arrived(ret.at[e], ret_s.at[e], ret_r.at[e], me != e)
-        combine = jnp.where(pos[:, e : e + 1] == slot_iota, share[:, e : e + 1], 0.0)
+        combine = jnp.where(route_t[0, e : e + 1, :] == slot_iota, route_t[1, e : e + 1, :], 0.0)
         high = combine.astype(BF16)
         low = (combine - high.astype(F32)).astype(BF16)
         back = ret[e]
-        total += jnp.dot(high, back, preferred_element_type=F32)
-        total += jnp.dot(low, back, preferred_element_type=F32)
+        total += lax.dot_general(high, back, over_slots, preferred_element_type=F32)
+        total += lax.dot_general(low, back, over_slots, preferred_element_type=F32)
     routed_ref[...] = total.astype(BF16)
 
     for make, cond in pending:
@@ -565,7 +571,6 @@
     down_cols = down_weight.shape[2]
     nk = 4
     n_z = n_ep // 2
-    ids_t = jnp.pad(route_ids.T, ((0, 0), (0, up_to(n_rows, 128) - n_rows)), constant_values=-1)
     cfg = (n_ep, n_tp, conv_kernel.shape[0], nk, slot, experts)
     vmem = pl.BlockSpec(memory_space=pltpu.VMEM)
     hbm = pl.BlockSpec(memory_space=pl.ANY)
@@ -576,13 +581,15 @@
             jax.ShapeDtypeStruct((length, cols_out), BF16),
             jax.ShapeDtypeStruct((n_rows, down_cols), BF16),
         ),
-        in_specs=[vmem] * 10 + [hbm] * 4,
+        in_specs=[vmem] * 9 + [hbm] * 4,
         out_specs=(vmem, vmem),
         scratch_shapes=[
             pltpu.VMEM((ch // 128, HALO + length, 128), F32),
             pltpu.VMEM((n_tp, length, ch), BF16),
             pltpu.VMEM((length // nk, n_tp * ch), BF16),
-            pltpu.VMEM((n_z, 2, n_rows + extra, width), BF16),
+            pltpu.VMEM((n_z, 2, n_rows, width), BF16),
+            pltpu.VMEM((n_ep, extra, n_rows), BF16),
+            pltpu.VMEM((2, extra, n_rows), F32),
             pltpu.VMEM((2 * slot, width), BF16),
             pltpu.VMEM((n_tp, n_z, 2 * slot, half_ff), BF16),
             pltpu.VMEM((n_z, 2 * slot, down_cols), BF16),
@@ -597,6 +604,8 @@
             dma((n_tp, nk)),
             dma((n_z, 3)),
             dma((n_z, 2)),
+            dma((n_ep,)),
+            dma((n_ep,)),
             dma((3, n_z, 2)),
             dma((n_tp, n_z, 2)),
             dma((n_ep,)),
@@ -609,13 +618,12 @@
         value_in,
         gate_in,
         conv_kernel,
-        norm_gain.reshape(n_tp, ch),
-        norm_shift.reshape(n_tp, ch),
+        norm_gain.reshape(1, n_tp * ch),
+        norm_shift.reshape(1, n_tp * ch),
         expert_input,
         expert_gain.reshape(1, width),
-        route_ids,
-        ids_t,
-        route_weights,
+        route_ids.T,
+        route_weights.T,
         out_weight,
         gate_weight,
         up_weight,

time: 109 us -> 103 us (0.945)
  local copies, waits for them, and re-layouts: 9.76 us -> 5.57 us
  Pallas kernels: 98.2 us -> 96.7 us
    unnamed x6 -> x4, local copies, waits for them, and re-layouts: 5.88 us -> 2.98 us
    pallas_call x1, Pallas kernels: 98.2 us -> 96.7 us  [body(): pl.pallas_call(functools.partial(kernel, cfg), out_shape=(jax.ShapeDtypeS...]
    pad x1 -> x0, local copies, waits for them, and re-layouts: 1.28 us -> none  [body(): jnp.pad(route_ids.T, ((0, 0), (0, up_to(n_rows, 128) - n_rows)), constant...]
where the time goes in v2:
time: 103 us
  Pallas kernels  96.7 us (94%)
  local copies, waits for them, and re-layouts  5.57 us (5%)
    pallas_call x1, Pallas kernels, body(): pl.pallas_call(functools.partial(kernel, cfg), out_shape=(jax.ShapeDtypeS...  96.7 us
    unnamed x4, local copies, waits for them, and re-layouts  2.98 us

profile of v2, /device:TPU:1, one launch (start us, length us, event | category | flops | bytes accessed | tf_op | source)
XLA Modules:
  0.0 102.9 jit_solution(3857755384390888422)
XLA Ops:
  0.6 1.3 %reshape.13.gain_ref = f32[1,1536]{1,0:T(1,128)} reshape(f32[1536]{0:T(1024)} %param.16) | data formatting | bytes 12288 | tf_op jit(solution)/shard_map/reshape | solution.py:621
  1.9 1.3 %reshape.14.shift_ref = f32[1,1536]{1,0:T(1,128)} reshape(f32[1536]{0:T(1024)} %param.17) | data formatting | bytes 12288 | tf_op jit(solution)/shard_map/reshape | solution.py:622
  3.2 96.7 %shard_map.140 = (bf16[1024,512]{1,0:T(8,128)(2,1)}, bf16[192,512]{1,0:T(8,128)(2,1)}) custom-call(bf16[1024,384]{1,0:T(8,128)(2,1)} %value_ref.1, bf16[1024,384]{1,0:T(8,128)(2,1)} %gate_ref.1, f32[31,384]{1,0:T(8,128)} %taps_ref.1, f32[1,1536]{1,0:T(1,128)} %reshape.13.gain_ref, f32[1,1536]{1,0:T(1,128)} %reshape.14.shift_ref, bf16[192,2048]{1,0:T(8,128)(2,1)} %rows_ref.1, ...), custom_call_target="tpu_custom_call" | custom-call | tf_op jit(solution)/shard_map/pallas_call | solution.py:578
  99.9 0.0 copy-start
  99.9 2.3 %copy.17 = bf16[1024,512]{1,0:T(8,128)(2,1)} copy(bf16[1024,512]{1,0:T(8,128)(2,1)} %get-tuple-element.4) | data formatting | bytes 2097152
  102.2 0.0 copy-done
  102.2 0.7 copy.18
Async XLA Ops:
  99.9 2.3 %copy-start = (bf16[192,512]{1,0:T(8,128)(2,1)S(1)}, bf16[192,512]{1,0:T(8,128)(2,1)}, u32[]{:S(2)}) copy-start(bf16[192,512]{1,0:T(8,128)(2,1)} %get-tuple-element.5) | copy-start | bytes 589828
